TPU v7x, 1024 devices: a whole 4x4x32 slice. The times are simulated.
1024 devices in a mesh: rep: 4 (over z_hi), fs: 32 (over z_lo, y), tp: 8 (over x, core).
Axes of the slice: x: 4, y: 4, z: 32 (z_hi: 4, z_lo: 8; z = z_hi * 8 + z_lo), core: 2. Of those that a mesh axis runs over, the one named last changes fastest.
Arguments:
- hidden_pre: bfloat16 [65536, 4096], P(('rep', 'fs'), 'tp'), may hold values from -6 to 6
- out_grad: bfloat16 [65536, 2048], P(('rep', 'fs')), may hold values from -24 to 24
- down_weight: bfloat16 [2048, 4096], P('fs', 'tp'), may hold values from -0.09375 to 0.09375
Outputs:
- hidden_grad: bfloat16 [65536, 4096], P(('rep', 'fs'), 'tp')
- weight_grad: float32 [2048, 4096], P('fs', 'tp')
All inputs are finite; a program needn't handle non-finite values.
Results may differ from a plain program's by a relative error of at most 0.0049.
Values may be sent and summed in bfloat16 or wider, within the bound.
A program may use at most 32 MiB of HBM per device.

v0:
```python
import math

import jax
import jax.numpy as jnp
from jax import lax
from jax.sharding import PartitionSpec as P


def body(hidden_pre, out_grad, down_weight):
    rows = hidden_pre.shape[0]
    ff_local = hidden_pre.shape[1]
    back = jnp.dot(
        out_grad,
        lax.all_gather(down_weight, "fs", axis=0, tiled=True),
        preferred_element_type=jnp.float32,
    )
    positive = jnp.maximum(hidden_pre.astype(jnp.float32), 0.0)
    hidden_grad = (2.0 * positive * back).astype(jnp.bfloat16)
    act = (positive * positive).astype(jnp.bfloat16)
    partial_value = lax.dot_general(
        out_grad, act, (((0,), (0,)), ((), ())), preferred_element_type=jnp.float32
    )
    partial_value = partial_value.astype(jnp.bfloat16)
    received = lax.all_to_all(partial_value, "fs", split_axis=0, concat_axis=0, tiled=True)
    groups = lax.axis_size("fs")
    local_sum = jnp.sum(
        received.reshape(groups, received.shape[0] // groups, ff_local), axis=0, dtype=jnp.float32
    )
    total = lax.psum(local_sum, "rep")
    tokens_all = rows * lax.axis_size("rep") * groups
    weight_grad = total * (1.0 / math.sqrt(tokens_all))
    return (hidden_grad, weight_grad)


def solution(mesh):
    placed = (P(("rep", "fs"), "tp"), P(("rep", "fs"), None), P("fs", "tp"))
    return jax.shard_map(
        body,
        mesh=mesh,
        in_specs=placed,
        out_specs=(P(("rep", "fs"), "tp"), P("fs", "tp")),
        check_vma=False,
    )
```

profile of v0, /device:TPU:6, one launch (start us, length us, event | category | flops | bytes accessed | tf_op | source)
XLA Modules:
  0.0 287.4 jit_solution(5262767015886588108)
XLA Ops:
  8.0 0.0 copy-start
  8.0 1.6 copy-done
  9.6 3.7 %fusion = bf16[2048,512]{0,1:T(8,128)(2,1)} fusion(bf16[512,2048]{1,0:T(8,128)(2,1)S(1)} %copy-done, bf16[512,512]{1,0:T(8,128)(2,1)} %param.3), kind=kOutput, calls=%fused_computation.2 | convolution fusion | flops 1075838976 | bytes 4718592 | tf_op jit(solution)/shard_map/dot_general | solution.py:20
  13.2 3.9 %copy.5 = bf16[2048,512]{1,0:T(8,128)(2,1)} copy(bf16[2048,512]{0,1:T(8,128)(2,1)} %fusion) | data formatting | bytes 4194304 | tf_op jit(solution)/shard_map/convert_element_type | solution.py:23
  17.2 15.7 %all-to-all-start = ((bf16[32,64,512]{2,1,0:T(8,128)(2,1)}), bf16[32,64,512]{2,1,0:T(8,128)(2,1)}, u32[]{:S(2)}, u32[]{:S(2)}) async-start(bf16[32,64,512]{2,1,0:T(8,128)(2,1)} %bitcast.6), calls=%async_computation | async-start | bytes 4194304 | tf_op jit(solution)/shard_map/all_to_all | solution.py:24
  32.8 0.0 copy-start.1
  32.9 0.0 all-gather.2.cloned.1.call-start
  32.9 0.7 all-gather.2.cloned.1.call-update
  33.6 0.0 all-reduce.2.cloned.1.call-start
  33.6 103.6 %all-to-all-done = bf16[32,64,512]{2,1,0:T(8,128)(2,1)} async-done(((bf16[32,64,512]{2,1,0:T(8,128)(2,1)}), bf16[32,64,512]{2,1,0:T(8,128)(2,1)}, u32[]{:S(2)}, u32[]{:S(2)}) %all-to-all-start) | async-done | bytes 2097184 | tf_op jit(solution)/shard_map/all_to_all | solution.py:24
  137.2 2.5 convert_reduce_fusion
  139.8 0.0 all-reduce.2.cloned.1.call-update
  139.8 135.0 %all-gather.2.cloned.1.call-done = bf16[2048,512]{1,0:T(8,128)(2,1)} async-done(((bf16[64,512]{1,0:T(8,128)(2,1)}), bf16[2048,512]{1,0:T(8,128)(2,1)}) %all-gather.2.cloned.1.call-update) | async-done | bytes 2097168 | tf_op jit(solution)/shard_map/all_gather | solution.py:14
  274.8 0.0 copy-done.1
  274.8 3.6 %fusion.1 = bf16[512,512]{1,0:T(8,128)(2,1)} fusion(bf16[512,2048]{1,0:T(8,128)(2,1)S(1)} %copy-done, bf16[2048,512]{1,0:T(8,128)(2,1)} %all-gather.2.cloned.1.call-done, bf16[512,512]{1,0:T(8,128)(2,1)S(1)} %copy-done.1), kind=kOutput, calls=%fused_computation.4 | convolution fusion | flops 1075052544 | bytes 5242880 | tf_op jit(solution)/shard_map/dot_general | solution.py:12
  278.4 0.0 all-reduce.2.cloned.1.call-done
  278.4 1.6 broadcast_multiply_fusion
Async XLA Ops:
  8.0 1.6 copy-start
  17.2 120.0 %all-to-all-start = ((bf16[32,64,512]{2,1,0:T(8,128)(2,1)}), bf16[32,64,512]{2,1,0:T(8,128)(2,1)}, u32[]{:S(2)}, u32[]{:S(2)}) async-start(bf16[32,64,512]{2,1,0:T(8,128)(2,1)} %bitcast.6), calls=%async_computation | async-start | bytes 4194304 | tf_op jit(solution)/shard_map/all_to_all | solution.py:24
  32.8 241.9 %copy-start.1 = (bf16[512,512]{1,0:T(8,128)(2,1)S(1)}, bf16[512,512]{1,0:T(8,128)(2,1)}, u32[]{:S(2)}) copy-start(bf16[512,512]{1,0:T(8,128)(2,1)} %param.3) | copy-start | bytes 1572868
  32.9 241.9 %all-gather.2.cloned.1.call-start = ((), (), s32[]{:S(2)}) async-start(), calls=%async_computation.1 | async-start | bytes 2162688 | tf_op jit(solution)/shard_map/all_gather | solution.py:14
  33.6 244.8 %all-reduce.2.cloned.1.call-start = ((), (), s32[]{:S(2)}) async-start(), calls=%async_computation.2 | async-start | bytes 262144 | tf_op jit(solution)/shard_map/psum | solution.py:29
Sparse Core Ops, SparseCore 0:
  36.3 238.4 all-gather.1
Sparse Core Ops, SparseCore 1:
  139.9 104.5 all-reduce.1
where the time goes:
time: 288 us; the launch traced here: 287 us
  waiting for transfers between devices  239 us (83%)
  starting transfers between devices  15.8 us (5%)
  between operations  15.5 us (5%)
  matrix products  7.3 us (3%)
  local copies, waits for them, and re-layouts  5.51 us (2%)
  other arithmetic  4.12 us (1%)
    all_gather x1, waiting for transfers between devices, body(): lax.all_gather(down_weight, 'fs', axis=0, tiled=True)  135 us
    all_to_all x1, waiting for transfers between devices, body(): lax.all_to_all(partial_value, 'fs', split_axis=0, concat_axis=0, tiled=True)  104 us
    all_to_all x1, starting transfers between devices, body(): lax.all_to_all(partial_value, 'fs', split_axis=0, concat_axis=0, tiled=True)  15.7 us
  transfers between devices with their start and end apart: 3, of which 2 were waited for; matrix products, arithmetic and copies ran while one was open for 2% of the time, Pallas kernels for 0%

commit v1 on v0

v1 whole, which is shorter than its diff:
```python
import functools
import math

import jax
import jax.numpy as jnp
from jax import lax
from jax.experimental import pallas as pl
from jax.experimental.pallas import tpu as pltpu
from jax.sharding import PartitionSpec as P

MESH = pl.DeviceIdType.MESH
NY = 4
NK = 8
NP = 4
ZOFF = (3, -3, 2, -2, 1, -1)
F32 = jnp.float32
BF16 = jnp.bfloat16


def kernel(
    scale, nrep,
    hp_hbm, og_hbm, w_hbm, hg_ref, wo_ref,
    hp, og, ogt, act, part, arecv, bmerged, brecv, zsend, zrecv, qsend, qrecv, tsend, trecv, wall, back,
    lsem, as_, ar_, us_, ur_, ms_, mr_, zs_, zr_, qs_, qr_, ts_, tr_, gzs, gzr, gys, gyr, near4,
):
    nz = nrep * NK
    h = lax.axis_index("rep")
    f = lax.axis_index("fs")
    k = f // NY
    j = lax.rem(f, NY)
    z = h * NK + k
    rows = w_hbm.shape[0]
    cols = w_hbm.shape[1] // NP
    quarter = rows // nrep
    half = rows // 2
    j1, j2, j3 = lax.rem(j + 1, NY), lax.rem(j + 2, NY), lax.rem(j + 3, NY)

    def ydev(jj):
        return {"fs": k * NY + jj}

    def zdev(d):
        zz = lax.rem(z + d + nz, nz)
        return {"rep": zz // NK, "fs": lax.rem(zz, NK) * NY + j}

    def kk(d):
        return lax.rem(k + d + NK, NK)

    right, left = ydev(j1), ydev(j3)
    sends = []

    def send(src, dst, ss, rs, dev):
        c = pltpu.make_async_remote_copy(
            src_ref=src, dst_ref=dst, send_sem=ss, recv_sem=rs, device_id=dev, device_id_type=MESH
        )
        c.start()
        sends.append(c)

    def got(dst, rs):
        pltpu.make_async_remote_copy(
            src_ref=dst, dst_ref=dst, send_sem=rs, recv_sem=rs, device_id=right, device_id_type=MESH
        ).wait_recv()

    barrier = pltpu.get_barrier_semaphore()
    peers = [right, left] + [zdev(d) for d in (1, -1, 2, -2, 3, -3, 4, -4)]
    for peer in peers:
        pl.semaphore_signal(barrier, inc=1, device_id=peer, device_id_type=MESH)

    wide = NY * rows
    loads = []

    def load(src, dst, i):
        c = pltpu.make_async_copy(src, dst, lsem.at[i])
        c.start()
        loads.append(c)

    load(hp_hbm, hp, 0)
    for i in range(NK):
        load(og_hbm.at[:, pl.ds(i * wide, wide)], og.at[i], 1 + i)
    load(w_hbm, wall.at[k, j], 1 + NK)

    loads[0].wait()
    pos = jnp.maximum(hp[...].astype(F32), 0.0)
    act[...] = (pos * pos).astype(BF16)

    def comp_one(p, i):
        res = jnp.dot(
            ogt[i], act[:, p * cols:(p + 1) * cols], preferred_element_type=F32
        ).astype(BF16)
        for jj in range(NY):
            part[p, jj, i] = res[jj * rows:(jj + 1) * rows]

    def comp(p):
        @pl.loop(0, NK)
        def _(i):
            comp_one(p, i)

    for i in range(NK):
        loads[1 + i].wait()
        ogt[i] = og[i].T
    comp(0)
    loads[1 + NK].wait()
    pl.semaphore_wait(barrier, len(peers))
    for d in (4, -4):
        pl.semaphore_signal(near4.at[0], inc=1, device_id=zdev(d), device_id_type=MESH)

    lo, hi = pl.ds(0, NK // 2), pl.ds(NK // 2, NK // 2)

    def send_a(p):
        send(part.at[p, j2, lo], arecv.at[p, 0], as_.at[p, 0], ar_.at[p, 0], right)
        send(part.at[p, j2, hi], arecv.at[p, 1], as_.at[p, 1], ar_.at[p, 1], left)

    def send_u(p):
        send(part.at[p, j1, hi], brecv.at[p, 0, hi], us_.at[p, 0], ur_.at[p, 0], right)
        send(part.at[p, j3, lo], brecv.at[p, 1, lo], us_.at[p, 1], ur_.at[p, 1], left)

    def merge(p):
        got(arecv.at[p, 0], ar_.at[p, 0])
        bmerged[p, 0] = (part[p, j1, lo].astype(F32) + arecv[p, 0].astype(F32)).astype(BF16)
        send(bmerged.at[p, 0], brecv.at[p, 0, lo], ms_.at[p, 0], mr_.at[p, 0], right)
        got(arecv.at[p, 1], ar_.at[p, 1])
        bmerged[p, 1] = (part[p, j3, hi].astype(F32) + arecv[p, 1].astype(F32)).astype(BF16)
        send(bmerged.at[p, 1], brecv.at[p, 1, hi], ms_.at[p, 1], mr_.at[p, 1], left)

    def ysum(p, i):
        return part[p, j, i].astype(F32) + brecv[p, 0, i].astype(F32) + brecv[p, 1, i].astype(F32)

    def recv_b(p):
        got(brecv.at[p, 0, hi], ur_.at[p, 0])
        got(brecv.at[p, 1, lo], ur_.at[p, 1])
        got(brecv.at[p, 0, lo], mr_.at[p, 0])
        got(brecv.at[p, 1, hi], mr_.at[p, 1])

        @pl.loop(0, NK)
        def _(i):
            zsend[p, i] = ysum(p, i).astype(BF16)

        far = kk(4)
        send(zsend.at[p, far, pl.ds(half, half)], zrecv.at[p, 6, pl.ds(half, half)], zs_.at[p, 6], zr_.at[p, 6], zdev(4))
        send(zsend.at[p, far, pl.ds(0, half)], zrecv.at[p, 6, pl.ds(0, half)], zs_.at[p, 7], zr_.at[p, 7], zdev(-4))
        for s, d in enumerate(ZOFF):
            send(zsend.at[p, kk(d)], zrecv.at[p, s], zs_.at[p, s], zr_.at[p, s], zdev(d))

    def recv_z(p):
        got(zrecv.at[p, 6, pl.ds(half, half)], zr_.at[p, 6])
        got(zrecv.at[p, 6, pl.ds(0, half)], zr_.at[p, 7])
        for s in range(len(ZOFF)):
            got(zrecv.at[p, s], zr_.at[p, s])
        q = ysum(p, k)
        for s in range(len(ZOFF) + 1):
            q = q + zrecv[p, s].astype(F32)
        qsend[p] = q.astype(BF16)
        for r in range(nrep):
            send(
                qsend.at[p, pl.ds(r * quarter, quarter)], qrecv.at[p, h], qs_.at[p, r], qr_.at[p, h],
                {"rep": r, "fs": kk(4) * NY + j},
            )

    def recv_q(p):
        for r in range(nrep):
            got(qrecv.at[p, r], qr_.at[p, r])
        t = qrecv[p, 0].astype(F32)
        for r in range(1, nrep):
            t = t + qrecv[p, r].astype(F32)
        tsend[p] = (t * scale).astype(BF16)
        for r in range(nrep):
            send(tsend.at[p], trecv.at[p, h], ts_.at[p, r], tr_.at[p, h], {"rep": r, "fs": kk(4) * NY + j})

    def recv_t(p):
        for r in range(nrep):
            got(trecv.at[p, r], tr_.at[p, r])
            wo_ref[r * quarter:(r + 1) * quarter, p * cols:(p + 1) * cols] = trecv[p, r].astype(F32)

    def gz(s):
        lower, upper = kk(-s), kk(s)
        if s > 0:
            got(wall.at[lower, j], gzr.at[s - 1, 0])
            got(wall.at[upper, j], gzr.at[s - 1, 1])
        if s < NK // 2 - 1:
            send(wall.at[lower, j], wall.at[lower, j], gzs.at[s, 0], gzr.at[s, 0], zdev(1))
            send(wall.at[upper, j], wall.at[upper, j], gzs.at[s, 1], gzr.at[s, 1], zdev(-1))
        else:
            a = wall.at[lower, j, pl.ds(0, half)]
            b = wall.at[upper, j, pl.ds(half, half)]
            send(a, a, gzs.at[s, 0], gzr.at[s, 0], zdev(1))
            send(b, b, gzs.at[s, 1], gzr.at[s, 1], zdev(-1))

    def gy_own():
        far = kk(4)
        got(wall.at[far, j, pl.ds(0, half)], gzr.at[NK // 2 - 1, 0])
        got(wall.at[far, j, pl.ds(half, half)], gzr.at[NK // 2 - 1, 1])
        a, b = wall.at[lo, j], wall.at[hi, j]
        send(a, a, gys.at[0, 0], gyr.at[0, 0], right)
        send(b, b, gys.at[0, 1], gyr.at[0, 1], left)
        send(b, b, gys.at[1, 0], gyr.at[1, 0], right)
        send(a, a, gys.at[1, 1], gyr.at[1, 1], left)

    def gy_forward():
        a, b = wall.at[lo, j3], wall.at[hi, j1]
        got(a, gyr.at[0, 0])
        send(a, a, gys.at[2, 0], gyr.at[2, 0], right)
        got(b, gyr.at[0, 1])
        send(b, b, gys.at[2, 1], gyr.at[2, 1], left)

    def gy_done():
        got(wall.at[hi, j3], gyr.at[1, 0])
        got(wall.at[lo, j1], gyr.at[1, 1])
        got(wall.at[lo, j2], gyr.at[2, 0])
        got(wall.at[hi, j2], gyr.at[2, 1])

    send_a(0)
    send_u(0)
    gz(0)
    comp(1)
    send_a(1)
    merge(0)
    send_u(1)
    gz(1)
    comp(2)
    send_a(2)
    merge(1)
    send_u(2)
    pl.semaphore_wait(near4.at[0], 2)
    for d in (4, -4):
        pl.semaphore_signal(near4.at[1], inc=1, device_id=zdev(d), device_id_type=MESH)
    recv_b(0)
    gz(2)
    comp(3)
    send_a(3)
    merge(2)
    send_u(3)
    recv_b(1)
    pl.semaphore_wait(near4.at[1], 2)
    recv_z(0)
    gz(3)
    merge(3)
    gy_own()
    recv_b(2)
    recv_z(1)
    recv_q(0)
    recv_b(3)
    recv_z(2)
    recv_q(1)
    recv_z(3)
    recv_q(2)
    gy_forward()
    recv_t(0)
    recv_t(1)
    recv_q(3)
    recv_t(2)
    gy_done()

    back[...] = jnp.zeros_like(back)

    @pl.loop(0, NK)
    def _(i):
        back[...] += jnp.dot(
            og[i], wall[i].reshape(wide, wall.shape[-1]), preferred_element_type=F32
        )

    hg_ref[...] = (2.0 * jnp.maximum(hp[...].astype(F32), 0.0) * back[...]).astype(BF16)
    recv_t(3)
    for c in sends:
        c.wait_send()


def body(hidden_pre, out_grad, down_weight):
    tok, ff = hidden_pre.shape
    width = out_grad.shape[1]
    rows = down_weight.shape[0]
    nrep = lax.axis_size("rep")
    cols = ff // NP
    scale = 1.0 / math.sqrt(tok * nrep * lax.axis_size("fs"))
    dma = pltpu.SemaphoreType.DMA
    return pl.pallas_call(
        functools.partial(kernel, scale, nrep),
        out_shape=(
            jax.ShapeDtypeStruct((tok, ff), BF16),
            jax.ShapeDtypeStruct((rows, ff), F32),
        ),
        in_specs=[pl.BlockSpec(memory_space=pl.ANY)] * 3,
        out_specs=[pl.BlockSpec(memory_space=pltpu.VMEM)] * 2,
        scratch_shapes=[
            pltpu.VMEM((tok, ff), BF16),
            pltpu.VMEM((NK, tok, width // NK), BF16),
            pltpu.VMEM((NK, width // NK, tok), BF16),
            pltpu.VMEM((tok, ff), BF16),
            pltpu.VMEM((NP, NY, NK, rows, cols), BF16),
            pltpu.VMEM((NP, 2, NK // 2, rows, cols), BF16),
            pltpu.VMEM((NP, 2, NK // 2, rows, cols), BF16),
            pltpu.VMEM((NP, 2, NK, rows, cols), BF16),
            pltpu.VMEM((NP, NK, rows, cols), BF16),
            pltpu.VMEM((NP, NK - 1, rows, cols), BF16),
            pltpu.VMEM((NP, rows, cols), BF16),
            pltpu.VMEM((NP, nrep, rows // nrep, cols), BF16),
            pltpu.VMEM((NP, rows // nrep, cols), BF16),
            pltpu.VMEM((NP, nrep, rows // nrep, cols), BF16),
            pltpu.VMEM((NK, NY, rows, ff), BF16),
            pltpu.VMEM((tok, ff), F32),
            dma((NK + 2,)),
            dma((NP, 2)), dma((NP, 2)),
            dma((NP, 2)), dma((NP, 2)),
            dma((NP, 2)), dma((NP, 2)),
            dma((NP, 8)), dma((NP, 8)),
            dma((NP, nrep)), dma((NP, nrep)),
            dma((NP, nrep)), dma((NP, nrep)),
            dma((NK // 2, 2)), dma((NK // 2, 2)),
            dma((3, 2)), dma((3, 2)),
            pltpu.SemaphoreType.REGULAR((2,)),
        ],
        compiler_params=pltpu.CompilerParams(collective_id=0, has_side_effects=True),
    )(hidden_pre, out_grad, down_weight)


def solution(mesh):
    placed = (P(("rep", "fs"), "tp"), P(("rep", "fs"), None), P("fs", "tp"))
    return jax.shard_map(
        body,
        mesh=mesh,
        in_specs=placed,
        out_specs=(P(("rep", "fs"), "tp"), P("fs", "tp")),
        check_vma=False,
    )
```

time: 288 us -> 81.3 us (0.28)
  waiting for transfers between devices: 239 us -> 0 us
  Pallas kernels: 0 us -> 76.8 us
  starting transfers between devices: 15.8 us -> 0 us
  between operations: 15.5 us -> 0.64 us
  matrix products: 7.3 us -> 0 us
  other arithmetic: 4.12 us -> 0 us
    all_gather x1 -> x0, waiting for transfers between devices: 135 us -> none  [body(): lax.all_gather(down_weight, 'fs', axis=0, tiled=True)]
    all_to_all x1 -> x0, waiting for transfers between devices: 104 us -> none  [body(): lax.all_to_all(partial_value, 'fs', split_axis=0, concat_axis=0, tiled=True)]
    pallas_call x0 -> x1, Pallas kernels: none -> 76.8 us  [body(): pl.pallas_call(functools.partial(kernel, scale, nrep), out_shape=(jax.Sha...]
    all_to_all x1 -> x0, starting transfers between devices: 15.7 us -> none  [body(): lax.all_to_all(partial_value, 'fs', split_axis=0, concat_axis=0, tiled=True)]
    dot_general x2 -> x0, matrix products: 7.3 us -> none  [the longest x1 3.66 us: body(): lax.dot_general(out_grad, act, (((0,), (0,)), ((), ())), preferred_elemen...]
    convert_element_type x1 -> x0, local copies, waits for them, and re-layouts: 3.91 us -> none  [body(): partial_value = partial_value.astype(jnp.bfloat16)]
  transfers between devices with their start and end apart: 3 -> 0, of which waited for: 2 -> 0; matrix products, arithmetic and copies ran while one was open for 2% -> 0% of each run, Pallas kernels for 0% -> 0%
where the time goes in v1:
time: 81.3 us; the launch traced here: 80.9 us
  Pallas kernels  76.8 us (94%)
  local copies, waits for them, and re-layouts  3.44 us (4%)
    pallas_call x1, Pallas kernels, body(): pl.pallas_call(functools.partial(kernel, scale, nrep), out_shape=(jax.Sha...  76.8 us
    unnamed x2, local copies, waits for them, and re-layouts  3.44 us

profile of v1, /device:TPU:6, one launch (start us, length us, event | category | flops | bytes accessed | tf_op | source)
XLA Modules:
  0.0 80.9 jit_solution(12273594413791477315)
XLA Ops:
  0.6 76.8 %shard_map.50 = (bf16[512,512]{1,0:T(8,128)(2,1)}, f32[64,512]{1,0:T(8,128)}) custom-call(bf16[512,512]{1,0:T(8,128)(2,1)} %hp_hbm.1, bf16[512,2048]{1,0:T(8,128)(2,1)} %og_hbm.1, bf16[64,512]{1,0:T(8,128)(2,1)} %w_hbm.1), custom_call_target="tpu_custom_call" | custom-call | tf_op jit(solution)/shard_map/pallas_call | solution.py:274
  77.5 1.9 %copy.7 = bf16[512,512]{1,0:T(8,128)(2,1)} copy(bf16[512,512]{1,0:T(8,128)(2,1)} %get-tuple-element.4) | data formatting | bytes 1048576
  79.3 1.6 %copy.8 = f32[64,512]{1,0:T(8,128)} copy(f32[64,512]{1,0:T(8,128)} %get-tuple-element.5) | data formatting | bytes 262144

commit v2 on v1

v2 whole, which is shorter than its diff:
```python
import functools
import math

import jax
import jax.numpy as jnp
from jax import lax
from jax.experimental import pallas as pl
from jax.experimental.pallas import tpu as pltpu
from jax.sharding import PartitionSpec as P

MESH = pl.DeviceIdType.MESH
NY = 4
NK = 8
NP = 4
ZOFF = (3, -3, 2, -2, 1, -1)
F32 = jnp.float32
BF16 = jnp.bfloat16


PASSES = ((0, 0, 64, 2), (1, 0, 64, 2), (2, 0, 64, 1), (3, 0, 32, 1), (3, 32, 32, 1))


def kernel(
    scale, nrep,
    hp_hbm, og_hbm, w_hbm, hg_hbm, wo_hbm,
    hp, og, ogt, ogp, act, part, arecv, bmerged, brecv, zsend, zrecv, qsend, qrecv, tsend, trecv, orecv, wall, back, hg, wo,
    lsem, osem, as_, ar_, us_, ur_, ms_, mr_, zs_, zr_, qs_, qr_, ts_, tr_, gzs, gzr, gys, gyr, near4,
):
    nz = nrep * NK
    h = lax.axis_index("rep")
    f = lax.axis_index("fs")
    k = f // NY
    j = lax.rem(f, NY)
    z = h * NK + k
    tok = hp.shape[0]
    rows = w_hbm.shape[0]
    cols = w_hbm.shape[1] // NP
    half = rows // 2
    j1, j2, j3 = lax.rem(j + 1, NY), lax.rem(j + 2, NY), lax.rem(j + 3, NY)

    def ydev(jj):
        return {"fs": k * NY + jj}

    def zdev(d):
        zz = lax.rem(z + d + nz, nz)
        return {"rep": zz // NK, "fs": lax.rem(zz, NK) * NY + j}

    def kk(d):
        return lax.rem(k + d + NK, NK)

    right, left = ydev(j1), ydev(j3)
    sends = []

    def send(src, dst, ss, rs, dev):
        c = pltpu.make_async_remote_copy(
            src_ref=src, dst_ref=dst, send_sem=ss, recv_sem=rs, device_id=dev, device_id_type=MESH
        )
        c.start()
        sends.append(c)

    def got(dst, rs):
        pltpu.make_async_remote_copy(
            src_ref=dst, dst_ref=dst, send_sem=rs, recv_sem=rs, device_id=right, device_id_type=MESH
        ).wait_recv()

    barrier = pltpu.get_barrier_semaphore()
    peers = [right, left] + [zdev(d) for d in (1, -1, 2, -2, 3, -3, 4, -4)]
    for peer in peers:
        pl.semaphore_signal(barrier, inc=1, device_id=peer, device_id_type=MESH)

    wide = NY * rows
    loads = []

    def load(src, dst, i):
        c = pltpu.make_async_copy(src, dst, lsem.at[i])
        c.start()
        loads.append(c)

    load(hp_hbm, hp, 0)
    for i in range(NK):
        load(og_hbm.at[:, pl.ds(i * wide, wide)], og.at[i], 1 + i)
    load(w_hbm, wall.at[j, k], 1 + NK)

    def load_act():
        loads[0].wait()
        pos = jnp.maximum(hp[...].astype(F32), 0.0)
        act[...] = (pos * pos).astype(BF16)

    def load_og():
        for i in range(NK):
            loads[1 + i].wait()
            t = og[i].T
            for jj in range(NY):
                ogt[jj, i * rows:(i + 1) * rows] = t[jj * rows:(jj + 1) * rows]

    def comp(c2, jj):
        res = jnp.dot(
            ogt[jj], act[:, 2 * c2 * cols:2 * (c2 + 1) * cols], preferred_element_type=F32
        ).astype(BF16)
        for c in range(2):
            part[2 * c2 + c, jj] = res[:, c * cols:(c + 1) * cols].reshape(NK, rows, cols)

    def comp_all(c2):
        @pl.loop(0, NY)
        def _(jj):
            comp(c2, jj)

    def near(i):
        if i > 0:
            pl.semaphore_wait(near4.at[i - 1], 2)
        for d in (4, -4):
            pl.semaphore_signal(near4.at[i], inc=1, device_id=zdev(d), device_id_type=MESH)

    lo, hi = pl.ds(0, NK // 2), pl.ds(NK // 2, NK // 2)

    def send_a(p):
        c, r0, nr, _ = PASSES[p]
        rr = pl.ds(r0, nr)
        send(part.at[c, j2, lo, rr], arecv.at[c, 0, :, rr], as_.at[p, 0], ar_.at[p, 0], right)
        send(part.at[c, j2, hi, rr], arecv.at[c, 1, :, rr], as_.at[p, 1], ar_.at[p, 1], left)

    def send_u(p):
        c, r0, nr, _ = PASSES[p]
        rr = pl.ds(r0, nr)
        send(part.at[c, j1, hi, rr], brecv.at[c, 0, hi, rr], us_.at[p, 0], ur_.at[p, 0], right)
        send(part.at[c, j3, lo, rr], brecv.at[c, 1, lo, rr], us_.at[p, 1], ur_.at[p, 1], left)

    def merge(p):
        c, r0, nr, _ = PASSES[p]
        rr = pl.ds(r0, nr)
        got(arecv.at[c, 0, :, rr], ar_.at[p, 0])
        bmerged[c, 0, :, rr] = (part[c, j1, lo, rr].astype(F32) + arecv[c, 0, :, rr].astype(F32)).astype(BF16)
        send(bmerged.at[c, 0, :, rr], brecv.at[c, 0, lo, rr], ms_.at[p, 0], mr_.at[p, 0], right)
        got(arecv.at[c, 1, :, rr], ar_.at[p, 1])
        bmerged[c, 1, :, rr] = (part[c, j3, hi, rr].astype(F32) + arecv[c, 1, :, rr].astype(F32)).astype(BF16)
        send(bmerged.at[c, 1, :, rr], brecv.at[c, 1, hi, rr], ms_.at[p, 1], mr_.at[p, 1], left)

    def ysum(c, i, rr):
        return (
            part[c, j, i, rr].astype(F32) + brecv[c, 0, i, rr].astype(F32) + brecv[c, 1, i, rr].astype(F32)
        )

    def recv_b(p):
        c, r0, nr, _ = PASSES[p]
        rr = pl.ds(r0, nr)
        got(brecv.at[c, 0, hi, rr], ur_.at[p, 0])
        got(brecv.at[c, 1, lo, rr], ur_.at[p, 1])
        got(brecv.at[c, 0, lo, rr], mr_.at[p, 0])
        got(brecv.at[c, 1, hi, rr], mr_.at[p, 1])
        zsend[c, :, rr] = ysum(c, slice(None), rr).astype(BF16)
        far = kk(4)
        up, dn = pl.ds(r0, nr // 2), pl.ds(r0 + nr // 2, nr // 2)
        send(zsend.at[c, far, dn], zrecv.at[c, 6, dn], zs_.at[p, 6], zr_.at[p, 6], zdev(4))
        send(zsend.at[c, far, up], zrecv.at[c, 6, up], zs_.at[p, 7], zr_.at[p, 7], zdev(-4))
        for s, d in enumerate(ZOFF):
            send(zsend.at[c, kk(d), rr], zrecv.at[c, s, rr], zs_.at[p, s], zr_.at[p, s], zdev(d))

    def recv_z(p):
        c, r0, nr, mode = PASSES[p]
        rr = pl.ds(r0, nr)
        up, dn = pl.ds(r0, nr // 2), pl.ds(r0 + nr // 2, nr // 2)
        got(zrecv.at[c, 6, dn], zr_.at[p, 6])
        got(zrecv.at[c, 6, up], zr_.at[p, 7])
        for s in range(len(ZOFF)):
            got(zrecv.at[c, s, rr], zr_.at[p, s])
        q = ysum(c, k, rr)
        for s in range(len(ZOFF) + 1):
            q = q + zrecv[c, s, rr].astype(F32)
        if mode == 2:
            quarter = nr // nrep
            qsend[c] = q.astype(BF16)
            for r in range(nrep):
                send(
                    qsend.at[c, pl.ds(r * quarter, quarter)], qrecv.at[c, h], qs_.at[p, r], qr_.at[p, h],
                    {"rep": r, "fs": kk(4) * NY + j},
                )
        else:
            orecv[c, h, rr] = q.astype(BF16)
            for i in (2, 1, 3):
                send(
                    orecv.at[c, h, rr], orecv.at[c, h, rr], qs_.at[p, i], qr_.at[p, i],
                    {"rep": lax.rem(h + i, nrep)},
                )

    def recv_q(p):
        c = PASSES[p][0]
        for r in range(nrep):
            got(qrecv.at[c, r], qr_.at[p, r])
        t = qrecv[c, 0].astype(F32)
        for r in range(1, nrep):
            t = t + qrecv[c, r].astype(F32)
        tsend[c] = (t * scale).astype(BF16)
        for r in range(nrep):
            send(tsend.at[c], trecv.at[c, h], ts_.at[p, r], tr_.at[p, h], {"rep": r, "fs": kk(4) * NY + j})

    def recv_t(p):
        c, r0, nr, mode = PASSES[p]
        cc = slice(c * cols, (c + 1) * cols)
        if mode == 2:
            quarter = nr // nrep
            for r in range(nrep):
                got(trecv.at[c, r], tr_.at[p, r])
                wo[r * quarter:(r + 1) * quarter, cc] = trecv[c, r].astype(F32)
        else:
            rr = pl.ds(r0, nr)
            for i in (2, 1, 3):
                got(orecv.at[c, lax.rem(h - i + nrep, nrep), rr], qr_.at[p, i])
            t = orecv[c, 0, rr].astype(F32)
            for r in range(1, nrep):
                t = t + orecv[c, r, rr].astype(F32)
            wo[rr, cc] = t * scale

    def gz(s):
        lower, upper = kk(-s), kk(s)
        if s == 0:
            loads[1 + NK].wait()
        if s > 0:
            got(wall.at[j, lower], gzr.at[s - 1, 0])
            got(wall.at[j, upper], gzr.at[s - 1, 1])
        if s < NK // 2 - 1:
            send(wall.at[j, lower], wall.at[j, lower], gzs.at[s, 0], gzr.at[s, 0], zdev(1))
            send(wall.at[j, upper], wall.at[j, upper], gzs.at[s, 1], gzr.at[s, 1], zdev(-1))
        else:
            a = wall.at[j, lower, pl.ds(0, half)]
            b = wall.at[j, upper, pl.ds(half, half)]
            send(a, a, gzs.at[s, 0], gzr.at[s, 0], zdev(1))
            send(b, b, gzs.at[s, 1], gzr.at[s, 1], zdev(-1))

    def gy_own():
        far = kk(4)
        got(wall.at[j, far, pl.ds(0, half)], gzr.at[NK // 2 - 1, 0])
        got(wall.at[j, far, pl.ds(half, half)], gzr.at[NK // 2 - 1, 1])
        a, b = wall.at[j, lo], wall.at[j, hi]
        send(a, a, gys.at[0, 0], gyr.at[0, 0], right)
        send(b, b, gys.at[0, 1], gyr.at[0, 1], left)
        send(b, b, gys.at[1, 0], gyr.at[1, 0], right)
        send(a, a, gys.at[1, 1], gyr.at[1, 1], left)

    def gy_forward():
        a, b = wall.at[j3, lo], wall.at[j1, hi]
        got(a, gyr.at[0, 0])
        send(a, a, gys.at[2, 0], gyr.at[2, 0], right)
        got(b, gyr.at[0, 1])
        send(b, b, gys.at[2, 1], gyr.at[2, 1], left)

    def gy_near():
        got(wall.at[j3, hi], gyr.at[1, 0])
        got(wall.at[j1, lo], gyr.at[1, 1])

    def gy_far():
        got(wall.at[j2, lo], gyr.at[2, 0])
        got(wall.at[j2, hi], gyr.at[2, 1])

    def w_block(jj):
        return jnp.dot(ogp[jj], wall[jj].reshape(NK * rows, wall.shape[-1]), preferred_element_type=F32)

    def w_own():
        @pl.loop(0, NY)
        def _(jj):
            ogp[jj] = ogt[jj].T

        back[...] = w_block(j)

    def w_near():
        back[...] += w_block(j3)
        back[...] += w_block(j1)

    def w_far():
        hg[...] = (2.0 * jnp.maximum(hp[...].astype(F32), 0.0) * (back[...] + w_block(j2))).astype(BF16)
        c = pltpu.make_async_copy(hg, hg_hbm, osem.at[0])
        c.start()
        loads.append(c)

    load_act()
    load_og()
    comp(0, j2)
    pl.semaphore_wait(barrier, len(peers))
    send_a(0)
    comp(0, j1)
    comp(0, j3)
    send_u(0)
    send_a(1)
    near(0)
    gz(0)
    comp(0, j)
    comp_all(1)
    merge(0)
    send_u(1)
    send_a(2)
    gz(1)
    near(1)
    merge(1)
    send_u(2)
    send_a(3)
    recv_b(0)
    gz(2)
    near(2)
    merge(2)
    send_u(3)
    send_a(4)
    recv_b(1)
    gz(3)
    pl.semaphore_wait(near4.at[2], 2)
    recv_z(0)
    merge(3)
    send_u(4)
    recv_b(2)
    merge(4)
    gy_own()
    recv_z(1)
    recv_b(3)
    recv_b(4)
    recv_z(2)
    recv_z(3)
    recv_q(0)
    recv_z(4)
    w_own()
    gy_forward()
    recv_q(1)
    gy_near()
    w_near()
    recv_t(0)
    recv_t(2)
    gy_far()
    w_far()
    recv_t(1)
    recv_t(3)
    recv_t(4)
    c = pltpu.make_async_copy(wo, wo_hbm, osem.at[1])
    c.start()
    loads[2 + NK].wait()
    c.wait()
    for c in sends:
        c.wait_send()


def body(hidden_pre, out_grad, down_weight):
    tok, ff = hidden_pre.shape
    width = out_grad.shape[1]
    rows = down_weight.shape[0]
    nrep = lax.axis_size("rep")
    cols = ff // NP
    npass = len(PASSES)
    scale = 1.0 / math.sqrt(tok * nrep * lax.axis_size("fs"))
    dma = pltpu.SemaphoreType.DMA
    return pl.pallas_call(
        functools.partial(kernel, scale, nrep),
        out_shape=(
            jax.ShapeDtypeStruct((tok, ff), BF16),
            jax.ShapeDtypeStruct((rows, ff), F32),
        ),
        in_specs=[pl.BlockSpec(memory_space=pl.ANY)] * 3,
        out_specs=[pl.BlockSpec(memory_space=pl.ANY)] * 2,
        scratch_shapes=[
            pltpu.VMEM((tok, ff), BF16),
            pltpu.VMEM((NK, tok, width // NK), BF16),
            pltpu.VMEM((NY, width // NY, tok), BF16),
            pltpu.VMEM((NY, tok, width // NY), BF16),
            pltpu.VMEM((tok, ff), BF16),
            pltpu.VMEM((NP, NY, NK, rows, cols), BF16),
            pltpu.VMEM((NP, 2, NK // 2, rows, cols), BF16),
            pltpu.VMEM((NP, 2, NK // 2, rows, cols), BF16),
            pltpu.VMEM((NP, 2, NK, rows, cols), BF16),
            pltpu.VMEM((NP, NK, rows, cols), BF16),
            pltpu.VMEM((NP, NK - 1, rows, cols), BF16),
            pltpu.VMEM((NP, rows, cols), BF16),
            pltpu.VMEM((NP, nrep, rows // nrep, cols), BF16),
            pltpu.VMEM((NP, rows // nrep, cols), BF16),
            pltpu.VMEM((NP, nrep, rows // nrep, cols), BF16),
            pltpu.VMEM((NP, nrep, rows, cols), BF16),
            pltpu.VMEM((NY, NK, rows, ff), BF16),
            pltpu.VMEM((tok, ff), F32),
            pltpu.VMEM((tok, ff), BF16),
            pltpu.VMEM((rows, ff), F32),
            dma((NK + 2,)),
            dma((2,)),
            dma((npass, 2)), dma((npass, 2)),
            dma((npass, 2)), dma((npass, 2)),
            dma((npass, 2)), dma((npass, 2)),
            dma((npass, 8)), dma((npass, 8)),
            dma((npass, nrep)), dma((npass, nrep)),
            dma((npass, nrep)), dma((npass, nrep)),
            dma((NK // 2, 2)), dma((NK // 2, 2)),
            dma((3, 2)), dma((3, 2)),
            pltpu.SemaphoreType.REGULAR((3,)),
        ],
        compiler_params=pltpu.CompilerParams(collective_id=0, has_side_effects=True),
    )(hidden_pre, out_grad, down_weight)


def solution(mesh):
    placed = (P(("rep", "fs"), "tp"), P(("rep", "fs"), None), P("fs", "tp"))
    return jax.shard_map(
        body,
        mesh=mesh,
        in_specs=placed,
        out_specs=(P(("rep", "fs"), "tp"), P("fs", "tp")),
        check_vma=False,
    )
```

time: 81.3 us -> 76.1 us (0.936); the launches traced: 80.9 us -> 74.7 us
  Pallas kernels: 76.8 us -> 70.7 us
    pallas_call x1, Pallas kernels: 76.8 us -> 70.7 us  [body(): pl.pallas_call(functools.partial(kernel, scale, nrep), out_shape=(jax.Sha...]
where the time goes in v2:
time: 76.1 us; the launch traced here: 74.7 us
  Pallas kernels  70.7 us (93%)
  local copies, waits for them, and re-layouts  3.44 us (5%)
    pallas_call x1, Pallas kernels, body(): pl.pallas_call(functools.partial(kernel, scale, nrep), out_shape=(jax.Sha...  70.7 us
    unnamed x2, local copies, waits for them, and re-layouts  3.44 us

profile of v2, /device:TPU:6, one launch (start us, length us, event | category | flops | bytes accessed | tf_op | source)
XLA Modules:
  0.0 74.7 jit_solution(14050700333867536317)
XLA Ops:
  0.6 70.7 %shard_map.50 = (bf16[512,512]{1,0:T(8,128)(2,1)}, f32[64,512]{1,0:T(8,128)}) custom-call(bf16[512,512]{1,0:T(8,128)(2,1)} %hp_hbm.1, bf16[512,2048]{1,0:T(8,128)(2,1)} %og_hbm.1, bf16[64,512]{1,0:T(8,128)(2,1)} %w_hbm.1), custom_call_target="tpu_custom_call" | custom-call | tf_op jit(solution)/shard_map/pallas_call | solution.py:346
  71.3 1.9 %copy.7 = bf16[512,512]{1,0:T(8,128)(2,1)} copy(bf16[512,512]{1,0:T(8,128)(2,1)} %get-tuple-element.4) | data formatting | bytes 1048576
  73.2 1.6 %copy.8 = f32[64,512]{1,0:T(8,128)} copy(f32[64,512]{1,0:T(8,128)} %get-tuple-element.5) | data formatting | bytes 262144

commit v3 on v2

v3 whole, which is shorter than its diff:
```python
import functools
import math

import jax
import jax.numpy as jnp
from jax import lax
from jax.experimental import pallas as pl
from jax.experimental.pallas import tpu as pltpu
from jax.sharding import PartitionSpec as P

MESH = pl.DeviceIdType.MESH
NY = 4
NK = 8
NP = 4
VMEM_LIMIT = 32 * 1024 * 1024
F32 = jnp.float32
BF16 = jnp.bfloat16


PASSES = ((0, 0, 64, 2, 2), (1, 0, 64, 2, 2), (2, 0, 64, 1, 2), (3, 0, 32, 1, 1), (3, 32, 32, 1, 1))


def kernel(
    scale, nrep,
    hp_hbm, og_hbm, w_hbm, hg, wo,
    hp, og, ogt, ogp, act, part, arecv, bmerged, brecv, zsend, zpre, zrecv, zmerged, qsend, qrecv, tsend, trecv, orecv, wall, back,
    lsem, ys_, ar_, br_, zs_, zp_, zr_, qs_, qr_, ts_, tr_, gs, gzr, gyr, near4,
):
    nz = nrep * NK
    h = lax.axis_index("rep")
    f = lax.axis_index("fs")
    k = f // NY
    j = lax.rem(f, NY)
    z = h * NK + k
    tok = hp.shape[0]
    rows = w_hbm.shape[0]
    cols = w_hbm.shape[1] // NP
    half = rows // 2
    j1, j2, j3 = lax.rem(j + 1, NY), lax.rem(j + 2, NY), lax.rem(j + 3, NY)

    def ydev(jj):
        return {"fs": k * NY + jj}

    def zdev(d):
        zz = lax.rem(z + d + nz, nz)
        return {"rep": zz // NK, "fs": lax.rem(zz, NK) * NY + j}

    def kk(d):
        return lax.rem(k + d + NK, NK)

    right, left = ydev(j1), ydev(j3)

    def send(src, dst, ss, rs, dev):
        pltpu.make_async_remote_copy(
            src_ref=src, dst_ref=dst, send_sem=ss, recv_sem=rs, device_id=dev, device_id_type=MESH
        ).start()

    def got(dst, rs):
        pltpu.make_async_remote_copy(
            src_ref=dst, dst_ref=dst, send_sem=rs, recv_sem=rs, device_id=right, device_id_type=MESH
        ).wait_recv()

    def sent(src, ss):
        pltpu.make_async_remote_copy(
            src_ref=src, dst_ref=src, send_sem=ss, recv_sem=ss, device_id=right, device_id_type=MESH
        ).wait_send()

    barrier = pltpu.get_barrier_semaphore()
    peers = [right, left] + [zdev(d) for d in (1, -1, 2, -2, 3, -3, 4, -4)]
    for peer in peers:
        pl.semaphore_signal(barrier, inc=1, device_id=peer, device_id_type=MESH)

    wide = NY * rows
    loads = []

    def load(src, dst, i):
        c = pltpu.make_async_copy(src, dst, lsem.at[i])
        c.start()
        loads.append(c)

    load(hp_hbm, hp, 0)
    for i in range(NK):
        load(og_hbm.at[:, pl.ds(i * wide, wide)], og.at[i], 1 + i)
    load(w_hbm, wall.at[j, k], 1 + NK)

    def load_act():
        loads[0].wait()
        pos = jnp.maximum(hp[...].astype(F32), 0.0)
        act[...] = (pos * pos).astype(BF16)

    def load_og():
        for i in range(NK):
            loads[1 + i].wait()
            t = og[i].T
            for jj in range(NY):
                ogt[jj, i * rows:(i + 1) * rows] = t[jj * rows:(jj + 1) * rows]

    def comp(c2, jj):
        res = jnp.dot(
            ogt[jj], act[:, 2 * c2 * cols:2 * (c2 + 1) * cols], preferred_element_type=F32
        ).astype(BF16)
        for c in range(2):
            part[2 * c2 + c, jj] = res[:, c * cols:(c + 1) * cols].reshape(NK, rows, cols)

    def comp_all(c2):
        @pl.loop(0, NY)
        def _(jj):
            comp(c2, jj)

    def near(i):
        if i > 0:
            pl.semaphore_wait(near4.at[i - 1], 2)
        for d in (4, -4):
            pl.semaphore_signal(near4.at[i], inc=1, device_id=zdev(d), device_id_type=MESH)

    lo, hi = pl.ds(0, NK // 2), pl.ds(NK // 2, NK // 2)

    def send_a(p):
        c, r0, nr = PASSES[p][:3]
        rr = pl.ds(r0, nr)
        send(part.at[c, j2, lo, rr], arecv.at[c, 0, :, rr], ys_.at[p], ar_.at[p, 0], right)
        send(part.at[c, j2, hi, rr], arecv.at[c, 1, :, rr], ys_.at[p], ar_.at[p, 1], left)

    def send_u(p):
        c, r0, nr = PASSES[p][:3]
        rr = pl.ds(r0, nr)
        send(part.at[c, j1, hi, rr], brecv.at[c, 0, hi, rr], ys_.at[p], br_.at[p], right)
        send(part.at[c, j3, lo, rr], brecv.at[c, 1, lo, rr], ys_.at[p], br_.at[p], left)

    def merge(p):
        c, r0, nr = PASSES[p][:3]
        rr = pl.ds(r0, nr)
        got(arecv.at[c, 0, :, rr], ar_.at[p, 0])
        bmerged[c, 0, :, rr] = (part[c, j1, lo, rr].astype(F32) + arecv[c, 0, :, rr].astype(F32)).astype(BF16)
        send(bmerged.at[c, 0, :, rr], brecv.at[c, 0, lo, rr], ys_.at[p], br_.at[p], right)
        got(arecv.at[c, 1, :, rr], ar_.at[p, 1])
        bmerged[c, 1, :, rr] = (part[c, j3, hi, rr].astype(F32) + arecv[c, 1, :, rr].astype(F32)).astype(BF16)
        send(bmerged.at[c, 1, :, rr], brecv.at[c, 1, hi, rr], ys_.at[p], br_.at[p], left)

    def ysum(c, i, rr):
        return (
            part[c, j, i, rr].astype(F32) + brecv[c, 0, i, rr].astype(F32) + brecv[c, 1, i, rr].astype(F32)
        )

    def recv_b(p):
        c, r0, nr = PASSES[p][:3]
        rr = pl.ds(r0, nr)
        got(brecv.at[c, :, :, rr], br_.at[p])
        zsend[c, :, rr] = ysum(c, slice(None), rr).astype(BF16)
        far = kk(4)
        up, dn = pl.ds(r0, nr // 2), pl.ds(r0 + nr // 2, nr // 2)
        if PASSES[p][4] == 1:
            send(zsend.at[c, far, dn], zrecv.at[c, 6, dn], zs_.at[p], zr_.at[p], zdev(4))
            send(zsend.at[c, far, up], zrecv.at[c, 6, up], zs_.at[p], zr_.at[p], zdev(-4))
            for i, d in enumerate((3, -3, 2, -2, 1, -1)):
                send(zsend.at[c, kk(d), rr], zrecv.at[c, i, rr], zs_.at[p], zr_.at[p], zdev(d))
            return
        for i, d in enumerate((1, -1)):
            hh = (dn, up)[i]
            send(zsend.at[c, kk(3 * d), rr], zpre.at[c, i, 0, rr], zs_.at[p], zp_.at[p, i], zdev(d))
            send(zsend.at[c, far, hh], zpre.at[c, i, 1, pl.ds(0, nr // 2)], zs_.at[p], zp_.at[p, 2 + i], zdev(2 * d))
        for i, d in enumerate((1, -1)):
            send(zsend.at[c, kk(d), rr], zrecv.at[c, i, rr], zs_.at[p], zr_.at[p], zdev(d))

    def merge_z(p):
        c, r0, nr = PASSES[p][:3]
        rr = pl.ds(r0, nr)
        up, dn = pl.ds(r0, nr // 2), pl.ds(r0 + nr // 2, nr // 2)
        for i, d in enumerate((1, -1)):
            got(zpre.at[c, i, 0, rr], zp_.at[p, i])
            m = ysum(c, kk(2 * d), rr) + zpre[c, i, 0, rr].astype(F32)
            got(zpre.at[c, i, 1, pl.ds(0, nr // 2)], zp_.at[p, 2 + i])
            zero = jnp.zeros((nr // 2, cols), F32)
            add = zpre[c, i, 1, pl.ds(0, nr // 2)].astype(F32)
            m = m + jnp.concatenate(((zero, add), (add, zero))[i], axis=0)
            zmerged[c, i, rr] = m.astype(BF16)
            send(zmerged.at[c, i, rr], zrecv.at[c, 2 + i, rr], zs_.at[p], zr_.at[p], zdev(2 * d))

    def recv_z(p):
        c, r0, nr, mode, _ = PASSES[p]
        rr = pl.ds(r0, nr)
        q = ysum(c, k, rr)
        many = (7, 4)[PASSES[p][4] - 1]
        got(zrecv.at[c, pl.ds(0, many), rr], zr_.at[p])
        for i in range(many):
            q = q + zrecv[c, i, rr].astype(F32)
        if mode == 2:
            quarter = nr // nrep
            qsend[c] = q.astype(BF16)
            for r in range(nrep):
                send(
                    qsend.at[c, pl.ds(r * quarter, quarter)], qrecv.at[c, h], qs_.at[p], qr_.at[p],
                    {"rep": r, "fs": kk(4) * NY + j},
                )
        else:
            orecv[c, h, rr] = q.astype(BF16)
            for i in (2, 1, 3):
                send(
                    orecv.at[c, h, rr], orecv.at[c, h, rr], qs_.at[p], qr_.at[p],
                    {"rep": lax.rem(h + i, nrep)},
                )

    def recv_q(p):
        c = PASSES[p][0]
        got(qrecv.at[c], qr_.at[p])
        t = qrecv[c, 0].astype(F32)
        for r in range(1, nrep):
            t = t + qrecv[c, r].astype(F32)
        tsend[c] = (t * scale).astype(BF16)
        for r in range(nrep):
            send(tsend.at[c], trecv.at[c, h], ts_.at[p], tr_.at[p], {"rep": r, "fs": kk(4) * NY + j})

    def recv_t(p):
        c, r0, nr, mode, _ = PASSES[p]
        cc = slice(c * cols, (c + 1) * cols)
        if mode == 2:
            quarter = nr // nrep
            got(trecv.at[c], tr_.at[p])
            for r in range(nrep):
                wo[r * quarter:(r + 1) * quarter, cc] = trecv[c, r].astype(F32)
        else:
            rr = pl.ds(r0, nr)
            got(orecv.at[c, pl.ds(0, nrep - 1), rr], qr_.at[p])
            t = orecv[c, 0, rr].astype(F32)
            for r in range(1, nrep):
                t = t + orecv[c, r, rr].astype(F32)
            wo[rr, cc] = t * scale

    def gz(s):
        lower, upper = kk(-s), kk(s)
        if s == 0:
            loads[1 + NK].wait()
        if s > 0:
            got(wall.at[j, lower], gzr.at[s - 1, 0])
            got(wall.at[j, upper], gzr.at[s - 1, 1])
        if s < NK // 2 - 1:
            send(wall.at[j, lower], wall.at[j, lower], gs.at[0], gzr.at[s, 0], zdev(1))
            send(wall.at[j, upper], wall.at[j, upper], gs.at[0], gzr.at[s, 1], zdev(-1))
        else:
            a = wall.at[j, lower, pl.ds(0, half)]
            b = wall.at[j, upper, pl.ds(half, half)]
            send(a, a, gs.at[0], gzr.at[s, 0], zdev(1))
            send(b, b, gs.at[0], gzr.at[s, 1], zdev(-1))

    def gy_own():
        far = kk(4)
        got(wall.at[j, far, pl.ds(0, half)], gzr.at[NK // 2 - 1, 0])
        got(wall.at[j, far, pl.ds(half, half)], gzr.at[NK // 2 - 1, 1])
        a, b = wall.at[j, lo], wall.at[j, hi]
        send(a, a, gs.at[1], gyr.at[0], right)
        send(b, b, gs.at[1], gyr.at[1], left)
        send(b, b, gs.at[1], gyr.at[2], right)
        send(a, a, gs.at[1], gyr.at[2], left)

    def gy_forward():
        a, b = wall.at[j3, lo], wall.at[j1, hi]
        got(a, gyr.at[0])
        send(a, a, gs.at[1], gyr.at[3], right)
        got(b, gyr.at[1])
        send(b, b, gs.at[1], gyr.at[3], left)

    def gy_near():
        got(wall.at[j], gyr.at[2])

    def gy_far():
        got(wall.at[j2], gyr.at[3])

    def w_block(jj):
        return jnp.dot(ogp[jj], wall[jj].reshape(NK * rows, wall.shape[-1]), preferred_element_type=F32)

    def w_own():
        @pl.loop(0, NY)
        def _(jj):
            ogp[jj] = ogt[jj].T

        back[...] = w_block(j)

    def w_near():
        back[...] += w_block(j3)
        back[...] += w_block(j1)

    def w_far():
        hg[...] = (2.0 * jnp.maximum(hp[...].astype(F32), 0.0) * (back[...] + w_block(j2))).astype(BF16)

    def st_sends():
        for p, (c, r0, nr, mode, _) in enumerate(PASSES):
            rr = pl.ds(r0, nr)
            sent(part.at[c, pl.ds(0, 3), :, rr], ys_.at[p])
            sent(zsend.at[c, pl.ds(0, NK - 1), rr], zs_.at[p])
            if mode == 2:
                sent(qsend.at[c], qs_.at[p])
                sent(trecv.at[c], ts_.at[p])
            else:
                sent(orecv.at[c, pl.ds(0, nrep - 1), rr], qs_.at[p])
        sent(wall.at[j, pl.ds(0, NK - 1)], gs.at[0])
        sent(wall.at[pl.ds(0, 3)], gs.at[1])

    load_act()
    load_og()
    comp(0, j2)
    pl.semaphore_wait(barrier, len(peers))
    send_a(0)
    comp(0, j1)
    comp(0, j3)
    send_u(0)
    send_a(1)
    near(0)
    gz(0)
    comp(0, j)
    comp_all(1)
    merge(0)
    send_u(1)
    send_a(2)
    gz(1)
    near(1)
    merge(1)
    send_u(2)
    send_a(3)
    recv_b(0)
    gz(2)
    near(2)
    merge(2)
    send_u(3)
    send_a(4)
    recv_b(1)
    merge_z(0)
    gz(3)
    pl.semaphore_wait(near4.at[2], 2)
    merge(3)
    send_u(4)
    recv_z(0)
    recv_b(2)
    merge_z(1)
    merge(4)
    gy_own()
    recv_b(3)
    recv_z(1)
    merge_z(2)
    recv_b(4)
    recv_z(3)
    recv_z(2)
    recv_z(4)
    recv_q(0)
    w_own()
    gy_forward()
    recv_q(1)
    gy_near()
    w_near()
    recv_t(0)
    recv_t(2)
    gy_far()
    w_far()
    recv_t(3)
    recv_t(4)
    recv_t(1)
    st_sends()


def body(hidden_pre, out_grad, down_weight):
    tok, ff = hidden_pre.shape
    width = out_grad.shape[1]
    rows = down_weight.shape[0]
    nrep = lax.axis_size("rep")
    cols = ff // NP
    npass = len(PASSES)
    scale = 1.0 / math.sqrt(tok * nrep * lax.axis_size("fs"))
    dma = pltpu.SemaphoreType.DMA
    hg, wo = pl.pallas_call(
        functools.partial(kernel, scale, nrep),
        out_shape=(pltpu.VMEM((tok, ff), BF16), pltpu.VMEM((rows, ff), F32)),
        in_specs=[pl.BlockSpec(memory_space=pltpu.HBM)] * 3,
        out_specs=[pl.BlockSpec(memory_space=pltpu.VMEM)] * 2,
        scratch_shapes=[
            pltpu.VMEM((tok, ff), BF16),
            pltpu.VMEM((NK, tok, width // NK), BF16),
            pltpu.VMEM((NY, width // NY, tok), BF16),
            pltpu.VMEM((NY, tok, width // NY), BF16),
            pltpu.VMEM((tok, ff), BF16),
            pltpu.VMEM((NP, NY, NK, rows, cols), BF16),
            pltpu.VMEM((NP, 2, NK // 2, rows, cols), BF16),
            pltpu.VMEM((NP, 2, NK // 2, rows, cols), BF16),
            pltpu.VMEM((NP, 2, NK, rows, cols), BF16),
            pltpu.VMEM((NP, NK, rows, cols), BF16),
            pltpu.VMEM((NP, 2, 2, rows, cols), BF16),
            pltpu.VMEM((NP, NK - 1, rows, cols), BF16),
            pltpu.VMEM((NP, 2, rows, cols), BF16),
            pltpu.VMEM((NP, rows, cols), BF16),
            pltpu.VMEM((NP, nrep, rows // nrep, cols), BF16),
            pltpu.VMEM((NP, rows // nrep, cols), BF16),
            pltpu.VMEM((NP, nrep, rows // nrep, cols), BF16),
            pltpu.VMEM((NP, nrep, rows, cols), BF16),
            pltpu.VMEM((NY, NK, rows, ff), BF16),
            pltpu.VMEM((tok, ff), F32),
            dma((NK + 2,)),
            dma((npass,)), dma((npass, 2)), dma((npass,)),
            dma((npass,)), dma((npass, 4)), dma((npass,)),
            dma((npass,)), dma((npass,)), dma((npass,)), dma((npass,)),
            dma((2,)), dma((NK // 2, 2)), dma((4,)),
            pltpu.SemaphoreType.REGULAR((3,)),
        ],
        compiler_params=pltpu.CompilerParams(collective_id=0, has_side_effects=True, vmem_limit_bytes=VMEM_LIMIT),
    )(*(pltpu.with_memory_space_constraint(x, pltpu.HBM) for x in (hidden_pre, out_grad, down_weight)))
    return hg, wo


def solution(mesh):
    placed = (P(("rep", "fs"), "tp"), P(("rep", "fs"), None), P("fs", "tp"))
    return jax.shard_map(
        body,
        mesh=mesh,
        in_specs=placed,
        out_specs=(P(("rep", "fs"), "tp"), P("fs", "tp")),
        check_vma=False,
    )
```

time: 76.1 us -> 71 us (0.933)
  Pallas kernels: 70.7 us -> 68.1 us
  local copies, waits for them, and re-layouts: 3.44 us -> 1.45 us
    pallas_call x1, Pallas kernels: 70.7 us -> 68.1 us  [body(): pl.pallas_call(functools.partial(kernel, scale, nrep), out_shape=(pltpu.V...]
    unnamed x2, local copies, waits for them, and re-layouts: 3.44 us -> 1.45 us
where the time goes in v3:
time: 71 us; the launch traced here: 70.2 us
  Pallas kernels  68.1 us (96%)
  local copies, waits for them, and re-layouts  1.45 us (2%)
    pallas_call x1, Pallas kernels, body(): pl.pallas_call(functools.partial(kernel, scale, nrep), out_shape=(pltpu.V...  68.1 us
    unnamed x2, local copies, waits for them, and re-layouts  1.45 us

profile of v3, /device:TPU:6, one launch (start us, length us, event | category | flops | bytes accessed | tf_op | source)
XLA Modules:
  0.0 70.2 jit_solution(9645106711567067905)
XLA Ops:
  0.6 68.1 %shard_map.50 = (bf16[512,512]{1,0:T(8,128)(2,1)S(1)}, f32[64,512]{1,0:T(8,128)S(1)}) custom-call(bf16[512,512]{1,0:T(8,128)(2,1)} %hp_hbm.1, bf16[512,2048]{1,0:T(8,128)(2,1)} %og_hbm.1, bf16[64,512]{1,0:T(8,128)(2,1)} %w_hbm.1), custom_call_target="tpu_custom_call" | custom-call | tf_op jit(solution)/shard_map/pallas_call | solution.py:368
  68.7 0.8 %copy.7 = bf16[512,512]{1,0:T(8,128)(2,1)} copy(bf16[512,512]{1,0:T(8,128)(2,1)S(1)} %get-tuple-element.2) | data formatting | bytes 1048576
  69.5 0.7 copy.8

commit v4 on v3

--- a/solution.py
+++ b/solution.py
@@ -17,14 +17,14 @@
 BF16 = jnp.bfloat16
 
 
-PASSES = ((0, 0, 64, 2, 2), (1, 0, 64, 2, 2), (2, 0, 64, 1, 2), (3, 0, 32, 1, 1), (3, 32, 32, 1, 1))
+PASSES = ((0, 0, 64, 2), (1, 0, 64, 2), (2, 0, 64, 2), (3, 0, 32, 1), (3, 32, 32, 1))
 
 
 def kernel(
     scale, nrep,
     hp_hbm, og_hbm, w_hbm, hg, wo,
-    hp, og, ogt, ogp, act, part, arecv, bmerged, brecv, zsend, zpre, zrecv, zmerged, qsend, qrecv, tsend, trecv, orecv, wall, back,
-    lsem, ys_, ar_, br_, zs_, zp_, zr_, qs_, qr_, ts_, tr_, gs, gzr, gyr, near4,
+    hp, og, ogt, ogp, act, part, arecv, bmerged, brecv, zsend, zpre, zrecv, zmerged, xq, xr, xt, xu, wall, back,
+    lsem, ys_, ar_, br_, zs_, zp_, zr_, xs_, xr_, xu_, gs, gzr, gyr, near4,
 ):
     nz = nrep * NK
     h = lax.axis_index("rep")
@@ -49,6 +49,8 @@
         return lax.rem(k + d + NK, NK)
 
     right, left = ydev(j1), ydev(j3)
+    turn = 8 - 16 * lax.rem(h, 2)
+    peer, other = zdev(turn), zdev(-turn)
 
     def send(src, dst, ss, rs, dev):
         pltpu.make_async_remote_copy(
@@ -67,8 +69,8 @@
 
     barrier = pltpu.get_barrier_semaphore()
     peers = [right, left] + [zdev(d) for d in (1, -1, 2, -2, 3, -3, 4, -4)]
-    for peer in peers:
-        pl.semaphore_signal(barrier, inc=1, device_id=peer, device_id_type=MESH)
+    for dev in peers:
+        pl.semaphore_signal(barrier, inc=1, device_id=dev, device_id_type=MESH)
 
     wide = NY * rows
     loads = []
@@ -149,7 +151,7 @@
         zsend[c, :, rr] = ysum(c, slice(None), rr).astype(BF16)
         far = kk(4)
         up, dn = pl.ds(r0, nr // 2), pl.ds(r0 + nr // 2, nr // 2)
-        if PASSES[p][4] == 1:
+        if PASSES[p][3] == 1:
             send(zsend.at[c, far, dn], zrecv.at[c, 6, dn], zs_.at[p], zr_.at[p], zdev(4))
             send(zsend.at[c, far, up], zrecv.at[c, 6, up], zs_.at[p], zr_.at[p], zdev(-4))
             for i, d in enumerate((3, -3, 2, -2, 1, -1)):
@@ -177,54 +179,30 @@
             send(zmerged.at[c, i, rr], zrecv.at[c, 2 + i, rr], zs_.at[p], zr_.at[p], zdev(2 * d))
 
     def recv_z(p):
-        c, r0, nr, mode, _ = PASSES[p]
-        rr = pl.ds(r0, nr)
+        c, r0, nr = PASSES[p][:3]
+        rr, up, dn = pl.ds(r0, nr), pl.ds(r0, nr // 2), pl.ds(r0 + nr // 2, nr // 2)
         q = ysum(c, k, rr)
-        many = (7, 4)[PASSES[p][4] - 1]
+        many = (7, 4)[PASSES[p][3] - 1]
         got(zrecv.at[c, pl.ds(0, many), rr], zr_.at[p])
         for i in range(many):
             q = q + zrecv[c, i, rr].astype(F32)
-        if mode == 2:
-            quarter = nr // nrep
-            qsend[c] = q.astype(BF16)
-            for r in range(nrep):
-                send(
-                    qsend.at[c, pl.ds(r * quarter, quarter)], qrecv.at[c, h], qs_.at[p], qr_.at[p],
-                    {"rep": r, "fs": kk(4) * NY + j},
-                )
-        else:
-            orecv[c, h, rr] = q.astype(BF16)
-            for i in (2, 1, 3):
-                send(
-                    orecv.at[c, h, rr], orecv.at[c, h, rr], qs_.at[p], qr_.at[p],
-                    {"rep": lax.rem(h + i, nrep)},
-                )
-
-    def recv_q(p):
-        c = PASSES[p][0]
-        got(qrecv.at[c], qr_.at[p])
-        t = qrecv[c, 0].astype(F32)
-        for r in range(1, nrep):
-            t = t + qrecv[c, r].astype(F32)
-        tsend[c] = (t * scale).astype(BF16)
-        for r in range(nrep):
-            send(tsend.at[c], trecv.at[c, h], ts_.at[p], tr_.at[p], {"rep": r, "fs": kk(4) * NY + j})
+        xq[c, rr] = q.astype(BF16)
+        send(xq.at[c, up], xr.at[c, up], xs_.at[p], xr_.at[p], peer)
+        send(xq.at[c, dn], xr.at[c, dn], xs_.at[p], xr_.at[p], other)
+
+    def recv_x(p):
+        c, r0, nr = PASSES[p][:3]
+        rr, up, dn = pl.ds(r0, nr), pl.ds(r0, nr // 2), pl.ds(r0 + nr // 2, nr // 2)
+        got(xr.at[c, rr], xr_.at[p])
+        xt[c, rr] = (xq[c, rr].astype(F32) + xr[c, rr].astype(F32)).astype(BF16)
+        send(xt.at[c, up], xu.at[c, up], xs_.at[p], xu_.at[p], other)
+        send(xt.at[c, dn], xu.at[c, dn], xs_.at[p], xu_.at[p], peer)
 
     def recv_t(p):
-        c, r0, nr, mode, _ = PASSES[p]
-        cc = slice(c * cols, (c + 1) * cols)
-        if mode == 2:
-            quarter = nr // nrep
-            got(trecv.at[c], tr_.at[p])
-            for r in range(nrep):
-                wo[r * quarter:(r + 1) * quarter, cc] = trecv[c, r].astype(F32)
-        else:
-            rr = pl.ds(r0, nr)
-            got(orecv.at[c, pl.ds(0, nrep - 1), rr], qr_.at[p])
-            t = orecv[c, 0, rr].astype(F32)
-            for r in range(1, nrep):
-                t = t + orecv[c, r, rr].astype(F32)
-            wo[rr, cc] = t * scale
+        c, r0, nr = PASSES[p][:3]
+        rr = pl.ds(r0, nr)
+        got(xu.at[c, rr], xu_.at[p])
+        wo[rr, c * cols:(c + 1) * cols] = (xt[c, rr].astype(F32) + xu[c, rr].astype(F32)) * scale
 
     def gz(s):
         lower, upper = kk(-s), kk(s)
@@ -283,15 +261,11 @@
         hg[...] = (2.0 * jnp.maximum(hp[...].astype(F32), 0.0) * (back[...] + w_block(j2))).astype(BF16)
 
     def st_sends():
-        for p, (c, r0, nr, mode, _) in enumerate(PASSES):
+        for p, (c, r0, nr, _) in enumerate(PASSES):
             rr = pl.ds(r0, nr)
             sent(part.at[c, pl.ds(0, 3), :, rr], ys_.at[p])
             sent(zsend.at[c, pl.ds(0, NK - 1), rr], zs_.at[p])
-            if mode == 2:
-                sent(qsend.at[c], qs_.at[p])
-                sent(trecv.at[c], ts_.at[p])
-            else:
-                sent(orecv.at[c, pl.ds(0, nrep - 1), rr], qs_.at[p])
+            sent(zsend.at[c, pl.ds(0, 2), rr], xs_.at[p])
         sent(wall.at[j, pl.ds(0, NK - 1)], gs.at[0])
         sent(wall.at[pl.ds(0, 3)], gs.at[1])
 
@@ -312,20 +286,18 @@
     send_u(1)
     send_a(2)
     gz(1)
-    near(1)
     merge(1)
     send_u(2)
     send_a(3)
     recv_b(0)
     gz(2)
-    near(2)
     merge(2)
     send_u(3)
     send_a(4)
     recv_b(1)
     merge_z(0)
     gz(3)
-    pl.semaphore_wait(near4.at[2], 2)
+    pl.semaphore_wait(near4.at[0], 2)
     merge(3)
     send_u(4)
     recv_z(0)
@@ -337,22 +309,25 @@
     recv_z(1)
     merge_z(2)
     recv_b(4)
+    recv_x(0)
     recv_z(3)
     recv_z(2)
     recv_z(4)
-    recv_q(0)
+    gy_forward()
+    recv_x(1)
     w_own()
-    gy_forward()
-    recv_q(1)
+    recv_x(3)
+    recv_x(2)
+    recv_x(4)
     gy_near()
     w_near()
     recv_t(0)
-    recv_t(2)
+    recv_t(1)
     gy_far()
     w_far()
     recv_t(3)
+    recv_t(2)
     recv_t(4)
-    recv_t(1)
     st_sends()
 
 
@@ -385,18 +360,17 @@
             pltpu.VMEM((NP, NK - 1, rows, cols), BF16),
             pltpu.VMEM((NP, 2, rows, cols), BF16),
             pltpu.VMEM((NP, rows, cols), BF16),
-            pltpu.VMEM((NP, nrep, rows // nrep, cols), BF16),
-            pltpu.VMEM((NP, rows // nrep, cols), BF16),
-            pltpu.VMEM((NP, nrep, rows // nrep, cols), BF16),
-            pltpu.VMEM((NP, nrep, rows, cols), BF16),
+            pltpu.VMEM((NP, rows, cols), BF16),
+            pltpu.VMEM((NP, rows, cols), BF16),
+            pltpu.VMEM((NP, rows, cols), BF16),
             pltpu.VMEM((NY, NK, rows, ff), BF16),
             pltpu.VMEM((tok, ff), F32),
             dma((NK + 2,)),
             dma((npass,)), dma((npass, 2)), dma((npass,)),
             dma((npass,)), dma((npass, 4)), dma((npass,)),
-            dma((npass,)), dma((npass,)), dma((npass,)), dma((npass,)),
+            dma((npass,)), dma((npass,)), dma((npass,)),
             dma((2,)), dma((NK // 2, 2)), dma((4,)),
-            pltpu.SemaphoreType.REGULAR((3,)),
+            pltpu.SemaphoreType.REGULAR((1,)),
         ],
         compiler_params=pltpu.CompilerParams(collective_id=0, has_side_effects=True, vmem_limit_bytes=VMEM_LIMIT),
     )(*(pltpu.with_memory_space_constraint(x, pltpu.HBM) for x in (hidden_pre, out_grad, down_weight)))

time: 71 us -> 68.6 us (0.966)
  Pallas kernels: 68.1 us -> 66.3 us
    pallas_call x1, Pallas kernels: 68.1 us -> 66.3 us  [body(): pl.pallas_call(functools.partial(kernel, scale, nrep), out_shape=(pltpu.V...]
where the time goes in v4:
time: 68.6 us; the launch traced here: 68.4 us
  Pallas kernels  66.3 us (97%)
  local copies, waits for them, and re-layouts  1.45 us (2%)
    pallas_call x1, Pallas kernels, body(): pl.pallas_call(functools.partial(kernel, scale, nrep), out_shape=(pltpu.V...  66.3 us
    unnamed x2, local copies, waits for them, and re-layouts  1.45 us

profile of v4, /device:TPU:6, one launch (start us, length us, event | category | flops | bytes accessed | tf_op | source)
XLA Modules:
  0.0 68.4 jit_solution(13327572467396423394)
XLA Ops:
  0.6 66.3 %shard_map.50 = (bf16[512,512]{1,0:T(8,128)(2,1)S(1)}, f32[64,512]{1,0:T(8,128)S(1)}) custom-call(bf16[512,512]{1,0:T(8,128)(2,1)} %hp_hbm.1, bf16[512,2048]{1,0:T(8,128)(2,1)} %og_hbm.1, bf16[64,512]{1,0:T(8,128)(2,1)} %w_hbm.1), custom_call_target="tpu_custom_call" | custom-call | tf_op jit(solution)/shard_map/pallas_call | solution.py:343
  66.9 0.8 %copy.7 = bf16[512,512]{1,0:T(8,128)(2,1)} copy(bf16[512,512]{1,0:T(8,128)(2,1)S(1)} %get-tuple-element.2) | data formatting | bytes 1048576
  67.7 0.7 copy.8
